TPU v7x, 32 devices: a whole 2x2x4 slice. The times are simulated.
32 devices in a mesh: ep: 8 (over z, x), tp: 4 (over y, core).
Axes of the slice: x: 2, y: 2, z: 4, core: 2. Of those that a mesh axis runs over, the one named last changes fastest.
Arguments:
- tokens: bfloat16 [768, 4096], P('ep'), may hold values from -6 to 6
- mix_gain: float32 [4096], replicated, may hold values from 0.1 to 1.9
- ffn_gain: float32 [4096], replicated, may hold values from 0.1 to 1.9
- in_proj: bfloat16 [4096, 1024], P(None, 'tp'), may hold values from -0.09375 to 0.09375
- decay_rate: float32 [64, 64], P('tp'), may hold values from 0.05 to 2
- frequency: float32 [64, 64], P('tp'), may hold values from -3 to 3
- log_step: float32 [64], P('tp'), may hold values from -3 to 0.5
- b_real: float32 [64, 64, 16], P('tp'), may hold values from -1.5 to 1.5
- b_imag: float32 [64, 64, 16], P('tp'), may hold values from -1.5 to 1.5
- c_real: float32 [64, 16, 64], P('tp'), may hold values from -0.75 to 0.75
- c_imag: float32 [64, 16, 64], P('tp'), may hold values from -0.75 to 0.75
- skip_gain: float32 [1024], P('tp'), may hold values from -5 to 5
- states: float32 [2, 768, 4096], P(None, 'ep', 'tp'), may hold values from -6 to 6
- out_proj: bfloat16 [1024, 4096], P('tp'), may hold values from -0.1875 to 0.1875
- route_ids: int32 [768, 2], P('ep'), may hold values from 0 to 7, all different within a row; in each aligned block of 96 rows (0 to 95, 96 to 191, ...) at most 48 rows name the same one
- route_logits: float32 [768, 2], P('ep'), may hold values from -5 to 5
- expert_gate: bfloat16 [8, 4096, 3072], P('ep', None, 'tp'), may hold values from -0.09375 to 0.09375
- expert_up: bfloat16 [8, 4096, 3072], P('ep', None, 'tp'), may hold values from -0.09375 to 0.09375
- expert_down: bfloat16 [8, 3072, 4096], P('ep', 'tp'), may hold values from -0.109375 to 0.109375
- dense_gate: bfloat16 [4096, 6144], P('tp', 'ep'), may hold values from -0.09375 to 0.09375
- dense_up: bfloat16 [4096, 6144], P('tp', 'ep'), may hold values from -0.09375 to 0.09375
- dense_down: bfloat16 [6144, 4096], P('ep', 'tp'), may hold values from -0.078125 to 0.078125
- branch_gate: bfloat16 [4096], replicated, may hold values from -0.09375 to 0.09375
Outputs:
- output: bfloat16 [768, 4096], P('ep', 'tp')
- new_states: float32 [2, 768, 4096], P(None, 'ep', 'tp')
Inputs may be any that keep to these rules, and one draw needn't show every extreme that they name: `route_ids`: each row names 2 different experts; among the rows of one device (aligned blocks of 96 rows) no expert is named by more than 48 rows.
All inputs are finite; a program needn't handle non-finite values.
Results may differ from a plain program's by a relative error of at most 0.017.
Values may be sent and summed in bfloat16 or wider, within the bound.
A program may use at most 128 MiB of HBM per device.

v0:
```python
import jax
import jax.numpy as jnp
from jax import lax
from jax.sharding import PartitionSpec as P

GROUP = 16
STATE = 64


def rms_norm(values, gain):
    flt = values.astype(jnp.float32)
    scaled = flt * lax.rsqrt(jnp.mean(flt * flt, axis=-1, keepdims=True) + 1e-06)
    return (scaled * gain).astype(jnp.bfloat16)


def discretize(decay_rate, frequency, log_step, b_real, b_imag):
    step_size = jnp.exp(log_step)[:, None]
    lam_re = -decay_rate
    magnitude = jnp.exp(lam_re * step_size)
    abar_re = magnitude * jnp.cos(frequency * step_size)
    abar_im = magnitude * jnp.sin(frequency * step_size)
    denom = lam_re * lam_re + frequency * frequency
    fac_re = ((abar_re - 1.0) * lam_re + abar_im * frequency) / denom
    fac_im = (abar_im * lam_re - (abar_re - 1.0) * frequency) / denom
    bbar_re = fac_re[..., None] * b_real - fac_im[..., None] * b_imag
    bbar_im = fac_re[..., None] * b_imag + fac_im[..., None] * b_real
    return (abar_re, abar_im, bbar_re, bbar_im)


def state_step(
    drive, states, decay_rate, frequency, log_step, b_real, b_imag, c_real, c_imag, skip_gain
):
    count = drive.shape[0]
    groups = decay_rate.shape[0]
    abar_re, abar_im, bbar_re, bbar_im = discretize(decay_rate, frequency, log_step, b_real, b_imag)
    grouped = drive.astype(jnp.float32).reshape(count, groups, GROUP)
    old_re = states[0].reshape(count, groups, STATE)
    old_im = states[1].reshape(count, groups, STATE)
    high = lax.Precision.HIGHEST
    push_re = jnp.einsum("ngh,gph->ngp", grouped, bbar_re, precision=high)
    push_im = jnp.einsum("ngh,gph->ngp", grouped, bbar_im, precision=high)
    new_re = abar_re * old_re - abar_im * old_im + push_re
    new_im = abar_re * old_im + abar_im * old_re + push_im
    readout = (
        jnp.einsum("ngp,ghp->ngh", new_re, c_real, precision=high)
        - jnp.einsum("ngp,ghp->ngh", new_im, c_imag, precision=high)
        + skip_gain.reshape(groups, GROUP) * grouped
    )
    reads = jax.nn.gelu(readout.reshape(count, groups * GROUP)).astype(jnp.bfloat16)
    fresh = jnp.stack(
        [new_re.reshape(count, groups * STATE), new_im.reshape(count, groups * STATE)]
    )
    return (reads, fresh)


def expert_rows(full_rows, gate_w, up_w, down_w, part_width):
    sources, items, width = full_rows.shape
    flat_rows = full_rows.reshape(sources * items, width)
    gate_val = jnp.dot(flat_rows, gate_w, preferred_element_type=jnp.float32)
    up_val = jnp.dot(flat_rows, up_w, preferred_element_type=jnp.float32)
    hidden = (jax.nn.silu(gate_val) * up_val).astype(jnp.bfloat16)
    partial_value = (
        jnp.dot(hidden, down_w, preferred_element_type=jnp.float32)
        .astype(jnp.bfloat16)
        .astype(jnp.float32)
    )
    summed = lax.psum_scatter(
        partial_value.astype(jnp.bfloat16), "tp", scatter_dimension=1, tiled=True
    )
    return summed.reshape(sources, items, part_width)


def shards(
    tokens,
    mix_gain,
    ffn_gain,
    in_proj,
    decay_rate,
    frequency,
    log_step,
    b_real,
    b_imag,
    c_real,
    c_imag,
    skip_gain,
    states,
    out_proj,
    route_ids,
    route_logits,
    expert_gate,
    expert_up,
    expert_down,
    dense_gate,
    dense_up,
    dense_down,
    branch_gate,
):
    seq_count, width = tokens.shape
    tp_count = lax.axis_size("tp")
    ep_count = lax.axis_size("ep")
    tp_index = lax.axis_index("tp")
    part_width = width // tp_count
    normed = rms_norm(tokens, mix_gain)
    drive = jnp.dot(normed, in_proj, preferred_element_type=jnp.float32).astype(jnp.bfloat16)
    reads, new_states = state_step(
        drive, states, decay_rate, frequency, log_step, b_real, b_imag, c_real, c_imag, skip_gain
    )
    partial_value = (
        jnp.dot(reads, out_proj, preferred_element_type=jnp.float32)
        .astype(jnp.bfloat16)
        .astype(jnp.float32)
    )
    mixed = lax.psum(partial_value.astype(jnp.bfloat16), "tp")
    resid = (tokens.astype(jnp.float32) + mixed.astype(jnp.float32)).astype(jnp.bfloat16)
    normed_two = rms_norm(resid, ffn_gain)
    own_cols = lax.dynamic_slice_in_dim(normed_two, tp_index * part_width, part_width, 1)
    hidden_width = dense_gate.shape[1]
    both_proj = jnp.concatenate([dense_gate, dense_up], axis=1)
    partial_both = jnp.dot(
        lax.all_gather(own_cols, "ep", axis=0, tiled=True),
        both_proj,
        preferred_element_type=jnp.float32,
    )
    summed_both = lax.psum(partial_both.astype(jnp.bfloat16), "tp").astype(jnp.float32)
    dense_hidden = (
        jax.nn.silu(summed_both[:, :hidden_width]) * summed_both[:, hidden_width:]
    ).astype(jnp.bfloat16)
    dense_term = lax.psum_scatter(
        jnp.dot(dense_hidden, dense_down, preferred_element_type=jnp.float32).astype(jnp.bfloat16),
        "ep",
        scatter_dimension=0,
        tiled=True,
    ).astype(jnp.float32)
    top_count = route_ids.shape[1]
    capacity = max(2, 2 * seq_count * top_count // ep_count)
    flat_ids = route_ids.reshape(-1)
    onehot = (flat_ids[:, None] == jnp.arange(ep_count, dtype=jnp.int32)[None, :]).astype(jnp.int32)
    rank = jnp.cumsum(onehot, axis=0) - onehot
    slot = jnp.sum(rank * onehot, axis=1)
    target = flat_ids * capacity + slot
    select = target[None, :] == jnp.arange(ep_count * capacity, dtype=jnp.int32)[:, None]
    select = jnp.any(select.reshape(ep_count * capacity, seq_count, top_count), axis=2).astype(
        jnp.bfloat16
    )
    send_rows = jnp.dot(select, normed_two, preferred_element_type=jnp.float32).astype(jnp.bfloat16)
    send_rows = send_rows.reshape(ep_count, capacity, width)
    send_part = lax.dynamic_slice_in_dim(send_rows, tp_index * part_width, part_width, 2)
    full_rows = lax.all_gather(
        lax.all_to_all(send_part, "ep", split_axis=0, concat_axis=0, tiled=True),
        "tp",
        axis=2,
        tiled=True,
    )
    answered = expert_rows(full_rows, expert_gate[0], expert_up[0], expert_down[0], part_width)
    returned = lax.all_to_all(answered, "ep", split_axis=0, concat_axis=0, tiled=True)
    picked_rows = returned.reshape(ep_count * capacity, part_width)[target]
    picked_rows = picked_rows.reshape(seq_count, top_count, part_width).astype(jnp.float32)
    route_weights = jax.nn.softmax(route_logits, axis=-1)
    routed = jnp.sum(route_weights[..., None] * picked_rows, axis=1)
    branch = jax.nn.sigmoid(jnp.dot(normed_two, branch_gate, preferred_element_type=jnp.float32))
    resid_cols = lax.dynamic_slice_in_dim(resid, tp_index * part_width, part_width, 1).astype(
        jnp.float32
    )
    output = (resid_cols + routed + branch[:, None] * dense_term).astype(jnp.bfloat16)
    return (output, new_states)


def solution(mesh):
    return jax.shard_map(
        shards,
        mesh=mesh,
        in_specs=(
            P("ep", None),
            P(),
            P(),
            P(None, "tp"),
            P("tp", None),
            P("tp", None),
            P("tp"),
            P("tp", None, None),
            P("tp", None, None),
            P("tp", None, None),
            P("tp", None, None),
            P("tp"),
            P(None, "ep", "tp"),
            P("tp", None),
            P("ep", None),
            P("ep", None),
            P("ep", None, "tp"),
            P("ep", None, "tp"),
            P("ep", "tp", None),
            P("tp", "ep"),
            P("tp", "ep"),
            P("ep", "tp"),
            P(),
        ),
        out_specs=(P("ep", "tp"), P(None, "ep", "tp")),
        check_vma=False,
    )
```

profile of v0, /device:TPU:0, one launch (start us, length us, event | category | flops | bytes accessed | tf_op | source)
XLA Modules:
  0.0 329.4 jit_solution(16527740815774029400)
XLA Ops:
  7.2 0.0 all-reduce.4.cloned.1.call-start
  7.2 1.4 exp.20
  8.7 2.1 fusion.69
  10.7 1.2 copy.42
  11.9 2.2 copy.43
  14.1 0.3 fusion.16
  14.4 2.8 convolution_convert_fusion.4
  17.2 0.9 copy.44
  18.1 0.8 add_divide_fusion
  18.9 1.9 fusion.26
  20.9 2.2 fusion.27
  23.1 0.1 mul.253
  23.1 1.5 fusion.70
  24.6 1.5 fusion.30
  26.1 0.1 fusion.49
  26.2 1.4 convolution_convert_fusion.1
  27.6 0.0 all-reduce.4.cloned.1.call-update
  27.6 0.0 all-gather.5.cloned.1.call-start
  27.6 0.1 copy.46
  27.7 0.1 eq.36
  27.9 37.6 %all-reduce.4.cloned.1.call-done = bf16[96,4096]{1,0:T(8,128)(2,1)} async-done(((bf16[96,4096]{1,0:T(8,128)(2,1)}), bf16[96,4096]{1,0:T(8,128)(2,1)}) %all-reduce.4.cloned.1.call-update) | async-done | bytes 786448 | tf_op jit(solution)/shard_map/psum | solution.py:113
  65.5 1.7 fusion.13
  67.3 0.9 copy-done.4
  68.1 0.3 fusion.15
  68.4 0.8 constant_dynamic-slice_fusion
  69.2 0.0 all-gather.5.cloned.1.call-update
  69.2 0.0 all-gather.3.cloned.1.call-start
  69.3 0.6 reduce-window.6
  69.9 0.2 slice_reduce_fusion
  70.1 0.1 add_bitcast_fusion
  70.3 0.6 copy-done.9
  70.8 0.8 reduce_sum.52
  71.6 0.8 broadcast_multiply_fusion
  72.4 0.1 copy.48
  72.5 0.1 fusion.41
  72.6 1.0 convolution_convert_fusion
  73.6 0.1 constant_dynamic-slice_fusion.1
  73.7 30.8 %all_to_all.10 = bf16[8,48,1024]{2,1,0:T(8,128)(2,1)} all-to-all(bf16[8,48,1024]{2,1,0:T(8,128)(2,1)S(1)} %constant_dynamic-slice_fusion.1), channel_id=1, replica_groups=mesh['ep'=8,'tp'=4] {'ep'}, dimensions={0} | all-to-all | bytes 1572864 | tf_op jit(solution)/shard_map/all_to_all | solution.py:149
  104.5 0.0 all-gather.3.cloned.1.call-update
  104.6 0.0 all-reduce.6.cloned.1.call-start
  104.6 14.9 %all-gather.5.cloned.1.call-done = bf16[768,1024]{1,0:T(8,128)(2,1)} async-done(((bf16[96,1024]{1,0:T(8,128)(2,1)}), bf16[768,1024]{1,0:T(8,128)(2,1)}) %all-gather.5.cloned.1.call-update) | async-done | bytes 1572880 | tf_op jit(solution)/shard_map/all_gather | solution.py:120
  119.5 6.4 %convolution_convert_fusion.2 = bf16[768,1536]{1,0:T(8,128)(2,1)} fusion(bf16[768,1024]{1,0:T(8,128)(2,1)} %all-gather.5.cloned.1.call-done, bf16[1024,768]{1,0:T(8,128)(2,1)} %param.43, bf16[1024,768]{1,0:T(8,128)(2,1)} %param.42), kind=kOutput, calls=%fused_computation.10 | convolution fusion | flops 2423390208 | bytes 7077888 | tf_op jit(solution)/shard_map/dot_general | solution.py:119
  125.9 0.2 reduce-scatter.3.cloned.1.call-start
  126.1 22.0 %all-gather.3.cloned.1.call-done = bf16[8,48,4096]{2,1,0:T(8,128)(2,1)} async-done(((bf16[8,48,1024]{2,1,0:T(8,128)(2,1)}), bf16[8,48,4096]{2,1,0:T(8,128)(2,1)}) %all-gather.3.cloned.1.call-update) | async-done | bytes 3145744 | tf_op jit(solution)/shard_map/all_gather | solution.py:148
  148.1 7.4 %fusion.4 = f32[384,768]{1,0:T(8,128)} fusion(bf16[384,4096]{1,0:T(8,128)(2,1)} %bitcast.89, bf16[1,4096,768]{2,1,0:T(8,128)(2,1)} %param.39), kind=kOutput, calls=%fused_computation.5 | convolution fusion | flops 2415919104 | bytes 10616832 | tf_op jit(solution)/shard_map/dot_general | solution.py:59
  155.5 14.3 %fusion.6 = bf16[384,4096]{1,0:T(8,128)(2,1)} fusion(bf16[1,768,4096]{2,1,0:T(8,128)(2,1)} %param.41, bf16[384,4096]{1,0:T(8,128)(2,1)} %bitcast.90, bf16[1,4096,768]{2,1,0:T(8,128)(2,1)} %param.40, f32[384,768]{1,0:T(8,128)} %fusion.4), kind=kOutput, calls=%fused_computation.8 | convolution fusion | flops 4835180544 | bytes 20054016 | tf_op jit(solution)/shard_map/dot_general | solution.py:63
  169.8 0.0 reduce-scatter.5.cloned.1.call-start
  169.9 36.2 %all-reduce.6.cloned.1.call-done = bf16[768,1536]{1,0:T(8,128)(2,1)} async-done(((bf16[768,1536]{1,0:T(8,128)(2,1)}), bf16[768,1536]{1,0:T(8,128)(2,1)}) %all-reduce.6.cloned.1.call-update) | async-done | bytes 2359312 | tf_op jit(solution)/shard_map/psum | solution.py:124
  206.0 2.4 convert_element_type.91
  208.5 2.6 convolution_convert_fusion.3
  211.1 35.2 %reduce-scatter.3.cloned.1.call-done = bf16[384,1024]{1,0:T(8,128)(2,1)} async-done(((bf16[384,4096]{1,0:T(8,128)(2,1)}), bf16[384,1024]{1,0:T(8,128)(2,1)}) %reduce-scatter.3.cloned.1.call-update) | async-done | bytes 786448 | tf_op jit(solution)/shard_map/reduce_scatter | solution.py:67
  246.2 5.5 %all-to-all-start.1 = ((bf16[8,48,1024]{2,1,0:T(8,128)(2,1)}), bf16[8,48,1024]{2,1,0:T(8,128)(2,1)S(1)}, u32[]{:S(2)}, u32[]{:S(2)}) async-start(bf16[8,48,1024]{2,1,0:T(8,128)(2,1)} %bitcast.86), calls=%async_computation.2 | async-start | bytes 1572864 | tf_op jit(solution)/shard_map/all_to_all | solution.py:155
  251.8 0.1 mul.275
  252.0 0.1 copy.45
  252.1 2.0 copy.50
  254.1 0.9 copy.49
  255.0 2.1 pad_maximum_fusion
  257.1 1.4 fusion.34
  258.5 22.2 %all-to-all-done.1 = bf16[8,48,1024]{2,1,0:T(8,128)(2,1)S(1)} async-done(((bf16[8,48,1024]{2,1,0:T(8,128)(2,1)}), bf16[8,48,1024]{2,1,0:T(8,128)(2,1)S(1)}, u32[]{:S(2)}, u32[]{:S(2)}) %all-to-all-start.1) | async-done | bytes 786464 | tf_op jit(solution)/shard_map/all_to_all | solution.py:155
  280.8 1.0 gather_fusion
  281.8 0.5 reshape.124
  282.3 1.0 multiply_reduce_fusion
  283.3 37.4 %reduce-scatter.5.cloned.1.call-done = bf16[96,1024]{1,0:T(8,128)(2,1)} async-done(((bf16[768,1024]{1,0:T(8,128)(2,1)}), bf16[96,1024]{1,0:T(8,128)(2,1)}) %reduce-scatter.5.cloned.1.call-update) | async-done | bytes 196624 | tf_op jit(solution)/shard_map/reduce_scatter | solution.py:128
  320.7 1.8 add_convert_fusion
  (50 shorter events, 0.3 us)
Async XLA Ops:
  7.2 19.0 %copy-start = (bf16[256,4096]{1,0:T(8,128)(2,1)S(1)}, bf16[256,4096]{1,0:T(8,128)(2,1)}, u32[]{:S(2)}) copy-start(bf16[256,4096]{1,0:T(8,128)(2,1)} %param.36) | copy-start | bytes 6291460
  7.2 6.9 %copy-start.5 = (bf16[96,4096]{1,0:T(8,128)(2,1)S(1)}, bf16[96,4096]{1,0:T(8,128)(2,1)}, u32[]{:S(2)}) copy-start(bf16[96,4096]{1,0:T(8,128)(2,1)} %param.23) | copy-start | bytes 2359300
  7.2 58.3 %all-reduce.4.cloned.1.call-start = ((), (), s32[]{:S(2)}) async-start(), calls=%async_computation.4 | async-start | bytes 1572864 | tf_op jit(solution)/shard_map/psum | solution.py:113
  11.9 7.0 %copy-start.2 = (f32[1,96,1024]{1,2,0:T(8,128)}, f32[1,96,1024]{1,2,0:T(8,128)S(1)}, u32[]{:S(2)}) copy-start(f32[1,96,1024]{1,2,0:T(8,128)S(1)} %copy.42) | copy-start | bytes 1179652
  14.1 4.0 %copy-start.12 = (f32[16,64]{1,0:T(8,128)S(1)}, f32[16,64]{1,0:T(8,128)}, u32[]{:S(2)}) copy-start(f32[16,64]{1,0:T(8,128)} %param.28) | copy-start | bytes 12292
  14.1 4.0 %copy-start.13 = (f32[16,64]{1,0:T(8,128)S(1)}, f32[16,64]{1,0:T(8,128)}, u32[]{:S(2)}) copy-start(f32[16,64]{1,0:T(8,128)} %param.27) | copy-start | bytes 12292
  14.1 4.8 %copy-start.6 = (f32[16,64,16]{1,2,0:T(8,128)S(1)}, f32[16,64,16]{1,2,0:T(8,128)}, u32[]{:S(2)}) copy-start(f32[16,64,16]{1,2,0:T(8,128)} %param.31) | copy-start | bytes 196612
  17.1 3.7 %copy-start.7 = (f32[16,64,16]{1,2,0:T(8,128)S(1)}, f32[16,64,16]{1,2,0:T(8,128)}, u32[]{:S(2)}) copy-start(f32[16,64,16]{1,2,0:T(8,128)} %param.30) | copy-start | bytes 196612
  17.2 5.9 %copy-start.15 = (f32[256]{0:T(256)S(1)}, f32[256]{0:T(256)}, u32[]{:S(2)}) copy-start(f32[256]{0:T(256)} %param.34) | copy-start | bytes 3076
  20.9 6.7 %copy-start.1 = (f32[96,16,64]{0,2,1:T(8,128)}, f32[96,16,64]{0,2,1:T(8,128)S(1)}, u32[]{:S(2)}) copy-start(f32[96,16,64]{0,2,1:T(8,128)S(1)} %fusion.26) | copy-start | bytes 1179652
  26.1 1.5 copy-start.16
  27.5 40.6 %copy-start.8 = (f32[4096]{0:T(1024)S(1)}, f32[4096]{0:T(1024)}, u32[]{:S(2)}) copy-start(f32[4096]{0:T(1024)} %param.25) | copy-start | bytes 49156
  27.6 91.9 %all-gather.5.cloned.1.call-start = ((), (), s32[]{:S(2)}) async-start(), calls=%async_computation.7 | async-start | bytes 1769472 | tf_op jit(solution)/shard_map/all_gather | solution.py:120
  67.2 0.9 copy-start.4
  68.4 5.2 %copy-start.3 = (bf16[96,4096]{1,0:T(8,128)(2,1)}, bf16[96,4096]{1,0:T(8,128)(2,1)S(1)}, u32[]{:S(2)}) copy-start(bf16[96,4096]{1,0:T(8,128)(2,1)S(1)} %fusion.15) | copy-start | bytes 2359300
  69.2 78.9 %all-gather.3.cloned.1.call-start = ((), (), s32[]{:S(2)}) async-start(), calls=%async_computation.5 | async-start | bytes 3932160 | tf_op jit(solution)/shard_map/all_gather | solution.py:148
  70.3 0.6 copy-start.9
  104.6 101.5 %all-reduce.6.cloned.1.call-start = ((), (), s32[]{:S(2)}) async-start(), calls=%async_computation.8 | async-start | bytes 4718592 | tf_op jit(solution)/shard_map/psum | solution.py:124
  125.9 120.4 %reduce-scatter.3.cloned.1.call-start = ((), (), s32[]{:S(2)}) async-start(), calls=%async_computation.6 | async-start | bytes 3932160 | tf_op jit(solution)/shard_map/reduce_scatter | solution.py:67
  169.8 150.9 %reduce-scatter.5.cloned.1.call-start = ((), (), s32[]{:S(2)}) async-start(), calls=%async_computation.9 | async-start | bytes 1769472 | tf_op jit(solution)/shard_map/reduce_scatter | solution.py:128
  206.0 2.4 copy-start.17
  211.0 40.9 %copy-start.11 = (f32[96,2]{0,1:T(2,128)S(1)}, f32[96,2]{0,1:T(2,128)}, u32[]{:S(2)}) copy-start(f32[96,2]{0,1:T(2,128)} %param.38) | copy-start | bytes 2308
  211.0 41.0 %copy-start.14 = (bf16[4096]{0:T(1024)(128)(2,1)S(1)}, bf16[4096]{0:T(1024)(128)(2,1)}, u32[]{:S(2)}) copy-start(bf16[4096]{0:T(1024)(128)(2,1)} %param.45) | copy-start | bytes 24580
  211.1 43.9 %copy-start.10 = (s32[192]{0:T(256)S(1)}, s32[192]{0:T(256)}, u32[]{:S(2)}) copy-start(s32[192]{0:T(256)} %copy-done.9) | copy-start | bytes 2308
  246.2 34.5 %all-to-all-start.1 = ((bf16[8,48,1024]{2,1,0:T(8,128)(2,1)}), bf16[8,48,1024]{2,1,0:T(8,128)(2,1)S(1)}, u32[]{:S(2)}, u32[]{:S(2)}) async-start(bf16[8,48,1024]{2,1,0:T(8,128)(2,1)} %bitcast.86), calls=%async_computation.2 | async-start | bytes 1572864 | tf_op jit(solution)/shard_map/all_to_all | solution.py:155
Sparse Core Ops, SparseCore 0:
  27.7 37.7 all-reduce.3
  69.3 50.0 all-gather.4
  121.0 27.0 all-gather.2
  150.3 55.6 all-reduce.5
  208.4 37.7 reduce-scatter.2
  249.5 71.1 reduce-scatter.4
where the time goes:
time: 330 us; the launch traced here: 329 us
  waiting for transfers between devices  205 us (62%)
  matrix products  44.3 us (13%)
  blocking collectives  30.8 us (9%)
  local copies, waits for them, and re-layouts  16.2 us (5%)
  between operations  14.4 us (4%)
  other arithmetic  12.1 us (4%)
  starting transfers between devices  5.94 us (2%)
    psum x1, waiting for transfers between devices, shards(): mixed = lax.psum(partial_value.astype(jnp.bfloat16), 'tp')  37.6 us
    reduce_scatter x1, waiting for transfers between devices, shards(): lax.psum_scatter(jnp.dot(dense_hidden, dense_down, preferred_element_type...  37.4 us
    psum x1, waiting for transfers between devices, shards(): lax.psum(partial_both.astype(jnp.bfloat16), 'tp').astype(jnp.float32)  36.2 us
    reduce_scatter x1, waiting for transfers between devices, expert_rows(): lax.psum_scatter(partial_value.astype(jnp.bfloat16), 'tp', scatter_dimens...  35.2 us
    all_to_all x1, blocking collectives, shards(): lax.all_to_all(send_part, 'ep', split_axis=0, concat_axis=0, tiled=True)  30.8 us
    all_to_all x1, waiting for transfers between devices, shards(): lax.all_to_all(answered, 'ep', split_axis=0, concat_axis=0, tiled=True)  22.2 us
    all_gather x1, waiting for transfers between devices, shards(): lax.all_gather(lax.all_to_all(send_part, 'ep', split_axis=0, concat_axis=...  22 us
    all_gather x1, waiting for transfers between devices, shards(): lax.all_gather(own_cols, 'ep', axis=0, tiled=True)  14.9 us
  transfers between devices with their start and end apart: 7, of which 7 were waited for; matrix products, arithmetic and copies ran while one was open for 14% of the time, Pallas kernels for 0%

commit v1 on v0

--- a/solution.py
+++ b/solution.py
@@ -5,6 +5,23 @@
 
 GROUP = 16
 STATE = 64
+
+
+def advance_spot(own_rows):
+    ax_name = "ep"
+    extra = jax.lax.axis_size(ax_name)
+    left_arr, known = (extra, jax.lax.axis_index(ax_name))
+    front = own_rows.shape[0] // left_arr
+    passed = jnp.roll(own_rows, -known * front, axis=0)
+    chunks = [lax.slice_in_dim(passed, 0, front, axis=0)]
+    for nth in range(1, left_arr):
+        block_last = lax.slice_in_dim(passed, nth * front, (nth + 1) * front, axis=0)
+        raw_out = jax.lax.ppermute(
+            block_last, ax_name, [(c, (c + nth) % left_arr) for c in range(left_arr)]
+        )
+        chunks.append(raw_out)
+    tile_out = jnp.concatenate(chunks[::-1], axis=0)
+    return jnp.roll(tile_out, shift=(known + 1) * chunks[0].shape[0], axis=0)
 
 
 def rms_norm(values, gain):
@@ -152,7 +169,7 @@
         tiled=True,
     )
     answered = expert_rows(full_rows, expert_gate[0], expert_up[0], expert_down[0], part_width)
-    returned = lax.all_to_all(answered, "ep", split_axis=0, concat_axis=0, tiled=True)
+    returned = advance_spot(answered)
     picked_rows = returned.reshape(ep_count * capacity, part_width)[target]
     picked_rows = picked_rows.reshape(seq_count, top_count, part_width).astype(jnp.float32)
     route_weights = jax.nn.softmax(route_logits, axis=-1)

time: 330 us -> 324 us (0.982)
  local copies, waits for them, and re-layouts: 16.2 us -> 7.75 us
  starting transfers between devices: 5.94 us -> 11 us
    all_to_all x1 -> x0, waiting for transfers between devices: 22.2 us -> none  [shards(): lax.all_to_all(answered, 'ep', split_axis=0, concat_axis=0, tiled=True)]
    ppermute x0 -> x7, waiting for transfers between devices: none -> 19.9 us  [advance_spot(): jax.lax.ppermute(block_last, ax_name, [(c, (c + nth) % left_arr) for c in...]
    ppermute x0 -> x7, starting transfers between devices: none -> 10.6 us  [advance_spot(): jax.lax.ppermute(block_last, ax_name, [(c, (c + nth) % left_arr) for c in...]
    all_to_all x1 -> x0, starting transfers between devices: 5.51 us -> none  [shards(): lax.all_to_all(answered, 'ep', split_axis=0, concat_axis=0, tiled=True)]
    reduce_scatter x1, waiting for transfers between devices: 35.2 us -> 31.5 us  [expert_rows(): lax.psum_scatter(partial_value.astype(jnp.bfloat16), 'tp', scatter_dimens...]
  transfers between devices with their start and end apart: 7 -> 13, of which waited for: 7 -> 10; matrix products, arithmetic and copies ran while one was open for 14% -> 14% of each run, Pallas kernels for 0% -> 0%
where the time goes in v1:
time: 324 us
  waiting for transfers between devices  203 us (63%)
  matrix products  43.9 us (14%)
  blocking collectives  30.8 us (10%)
  between operations  14.6 us (5%)
  other arithmetic  12.4 us (4%)
  starting transfers between devices  11 us (3%)
  local copies, waits for them, and re-layouts  7.75 us (2%)
    reduce_scatter x1, waiting for transfers between devices, shards(): lax.psum_scatter(jnp.dot(dense_hidden, dense_down, preferred_element_type...  39.4 us
    psum x1, waiting for transfers between devices, shards(): mixed = lax.psum(partial_value.astype(jnp.bfloat16), 'tp')  37.6 us
    psum x1, waiting for transfers between devices, shards(): lax.psum(partial_both.astype(jnp.bfloat16), 'tp').astype(jnp.float32)  36.2 us
    reduce_scatter x1, waiting for transfers between devices, expert_rows(): lax.psum_scatter(partial_value.astype(jnp.bfloat16), 'tp', scatter_dimens...  31.5 us
    all_to_all x1, blocking collectives, shards(): lax.all_to_all(send_part, 'ep', split_axis=0, concat_axis=0, tiled=True)  30.8 us
    all_gather x1, waiting for transfers between devices, shards(): lax.all_gather(lax.all_to_all(send_part, 'ep', split_axis=0, concat_axis=...  21.8 us
    ppermute x7, waiting for transfers between devices, advance_spot(): jax.lax.ppermute(block_last, ax_name, [(c, (c + nth) % left_arr) for c in...  19.9 us
    all_gather x1, waiting for transfers between devices, shards(): lax.all_gather(own_cols, 'ep', axis=0, tiled=True)  17.1 us
  transfers between devices with their start and end apart: 13, of which 10 were waited for; matrix products, arithmetic and copies ran while one was open for 14% of the time, Pallas kernels for 0%

profile of v1, /device:TPU:0, one launch (start us, length us, event | category | flops | bytes accessed | tf_op | source)
XLA Modules:
  0.0 323.9 jit_solution(3993747818430432152)
XLA Ops:
  7.2 0.8 exp.20
  8.0 1.2 fusion.72
  9.2 0.2 copy.42
  9.4 1.0 copy.43
  10.4 1.4 fusion.16
  11.9 2.4 convolution_convert_fusion.4
  14.3 0.1 copy.44
  14.4 0.1 add_divide_fusion
  14.6 1.8 fusion.26
  16.4 2.0 fusion.27
  18.4 0.1 mul.253
  18.5 1.5 fusion.73
  20.0 1.5 fusion.30
  21.5 0.1 fusion.51
  21.5 1.4 convolution_convert_fusion.1
  23.0 0.1 copy.46
  23.1 0.1 eq.38
  23.2 37.6 %all-reduce.4.cloned.1.call-done = bf16[96,4096]{1,0:T(8,128)(2,1)} async-done(((bf16[96,4096]{1,0:T(8,128)(2,1)}), bf16[96,4096]{1,0:T(8,128)(2,1)}) %all-reduce.4.cloned.1.call-update) | async-done | bytes 786448 | tf_op jit(solution)/shard_map/psum | solution.py:130
  60.8 1.7 fusion.13
  62.6 0.3 fusion.15
  62.9 0.7 constant_dynamic-slice_fusion
  63.7 0.6 reduce-window.6
  64.2 0.2 slice_reduce_fusion
  64.5 0.1 add_bitcast_fusion
  64.6 0.1 reduce_sum.52
  64.8 0.1 copy.48
  64.8 0.1 fusion.43
  65.0 1.0 convolution_convert_fusion
  66.0 0.1 constant_dynamic-slice_fusion.1
  66.1 30.8 %all_to_all.5 = bf16[8,48,1024]{2,1,0:T(8,128)(2,1)} all-to-all(bf16[8,48,1024]{2,1,0:T(8,128)(2,1)S(1)} %constant_dynamic-slice_fusion.1), channel_id=1, replica_groups=mesh['ep'=8,'tp'=4] {'ep'}, dimensions={0} | all-to-all | bytes 1572864 | tf_op jit(solution)/shard_map/all_to_all | solution.py:166
  96.9 17.1 %all-gather.5.cloned.1.call-done = bf16[768,1024]{1,0:T(8,128)(2,1)} async-done(((bf16[96,1024]{1,0:T(8,128)(2,1)}), bf16[768,1024]{1,0:T(8,128)(2,1)}) %all-gather.5.cloned.1.call-update) | async-done | bytes 1572880 | tf_op jit(solution)/shard_map/all_gather | solution.py:137
  114.0 6.4 %convolution_convert_fusion.2 = bf16[768,1536]{1,0:T(8,128)(2,1)} fusion(bf16[768,1024]{1,0:T(8,128)(2,1)} %all-gather.5.cloned.1.call-done, bf16[1024,768]{1,0:T(8,128)(2,1)} %param.45, bf16[1024,768]{1,0:T(8,128)(2,1)} %param.44), kind=kOutput, calls=%fused_computation.10 | convolution fusion | flops 2423390208 | bytes 7077888 | tf_op jit(solution)/shard_map/dot_general | solution.py:136
  120.4 0.2 reduce-scatter.3.cloned.1.call-start
  120.6 21.8 %all-gather.3.cloned.1.call-done = bf16[8,48,4096]{2,1,0:T(8,128)(2,1)} async-done(((bf16[8,48,1024]{2,1,0:T(8,128)(2,1)}), bf16[8,48,4096]{2,1,0:T(8,128)(2,1)}) %all-gather.3.cloned.1.call-update) | async-done | bytes 3145744 | tf_op jit(solution)/shard_map/all_gather | solution.py:165
  142.5 7.4 %fusion.4 = f32[384,768]{1,0:T(8,128)} fusion(bf16[384,4096]{1,0:T(8,128)(2,1)} %bitcast.89, bf16[1,4096,768]{2,1,0:T(8,128)(2,1)} %param.41), kind=kOutput, calls=%fused_computation.5 | convolution fusion | flops 2415919104 | bytes 10616832 | tf_op jit(solution)/shard_map/dot_general | solution.py:76
  149.8 14.3 %fusion.6 = bf16[384,4096]{1,0:T(8,128)(2,1)} fusion(bf16[1,768,4096]{2,1,0:T(8,128)(2,1)} %param.43, bf16[384,4096]{1,0:T(8,128)(2,1)} %bitcast.90, bf16[1,4096,768]{2,1,0:T(8,128)(2,1)} %param.42, f32[384,768]{1,0:T(8,128)} %fusion.4), kind=kOutput, calls=%fused_computation.8 | convolution fusion | flops 4835180544 | bytes 20054016 | tf_op jit(solution)/shard_map/dot_general | solution.py:80
  164.2 0.0 reduce-scatter.5.cloned.1.call-start
  164.2 36.2 %all-reduce.6.cloned.1.call-done = bf16[768,1536]{1,0:T(8,128)(2,1)} async-done(((bf16[768,1536]{1,0:T(8,128)(2,1)}), bf16[768,1536]{1,0:T(8,128)(2,1)}) %all-reduce.6.cloned.1.call-update) | async-done | bytes 2359312 | tf_op jit(solution)/shard_map/psum | solution.py:141
  200.4 2.3 convert_element_type.91
  202.7 4.0 %convolution_convert_fusion.3 = bf16[768,1024]{1,0:T(8,128)(2,1)} fusion(bf16[768,1024]{1,0:T(8,128)(2,1)} %param.46, f32[768,1536]{1,0:T(8,128)S(1)} %convert_element_type.91), kind=kOutput, calls=%fused_computation.21 | convolution fusion | flops 1212284928 | bytes 7864320 | tf_op jit(solution)/shard_map/dot_general | solution.py:146
  206.8 0.1 mul.275
  207.0 0.7 copy.45
  207.8 0.2 copy.50
  208.0 0.2 copy.49
  208.2 1.0 pad_maximum_fusion
  209.2 31.5 %reduce-scatter.3.cloned.1.call-done = bf16[384,1024]{1,0:T(8,128)(2,1)} async-done(((bf16[384,4096]{1,0:T(8,128)(2,1)}), bf16[384,1024]{1,0:T(8,128)(2,1)}) %reduce-scatter.3.cloned.1.call-update) | async-done | bytes 786448 | tf_op jit(solution)/shard_map/reduce_scatter | solution.py:84
  240.6 1.4 fusion.36
  242.0 0.1 fusion.71
  242.1 4.3 %collective-permute-start = (bf16[1,48,1024]{2,1,0:T(8,128)(2,1)S(1)}, bf16[1,48,1024]{2,1,0:T(8,128)(2,1)S(1)}, u32[]{:S(2)}, u32[]{:S(2)}) collective-permute-start(bf16[1,48,1024]{2,1,0:T(8,128)(2,1)S(1)} %get-tuple-element.11), channel_id=1, source_target_pairs={{0,28},{4,0},{8,4},{12,8},{16,12},{20,16},{24,20},{28,24},{1,29},{... | collective-permute-start | bytes 294920 | tf_op jit(solution)/shard_map/ppermute | solution.py:19
  246.4 0.3 fusion.34
  246.7 0.5 collective-permute-start.1
  247.2 3.0 collective-permute-start.3
  250.2 1.9 collective-permute-start.5
  252.1 0.4 collective-permute-done.1
  252.6 0.8 collective-permute-start.6
  253.4 2.5 collective-permute-done.2
  256.0 12.9 %collective-permute-done.3 = bf16[1,48,1024]{2,1,0:T(8,128)(2,1)S(1)} collective-permute-done((bf16[1,48,1024]{2,1,0:T(8,128)(2,1)S(1)}, bf16[1,48,1024]{2,1,0:T(8,128)(2,1)S(1)}, u32[]{:S(2)}, u32[]{:S(2)}) %collective-permute-start.3) | collective-permute-done | bytes 98336 | tf_op jit(solution)/shard_map/ppermute | solution.py:19
  268.9 4.0 %collective-permute-done.4 = bf16[1,48,1024]{2,1,0:T(8,128)(2,1)S(1)} collective-permute-done((bf16[1,48,1024]{2,1,0:T(8,128)(2,1)S(1)}, bf16[1,48,1024]{2,1,0:T(8,128)(2,1)S(1)}, u32[]{:S(2)}, u32[]{:S(2)}) %collective-permute-start.4) | collective-permute-done | bytes 98336 | tf_op jit(solution)/shard_map/ppermute | solution.py:19
  273.0 0.3 fusion.35
  273.3 1.0 gather_fusion
  274.3 0.5 reshape.124
  274.8 1.0 multiply_reduce_fusion
  275.9 39.4 %reduce-scatter.5.cloned.1.call-done = bf16[96,1024]{1,0:T(8,128)(2,1)} async-done(((bf16[768,1024]{1,0:T(8,128)(2,1)}), bf16[96,1024]{1,0:T(8,128)(2,1)}) %reduce-scatter.5.cloned.1.call-update) | async-done | bytes 196624 | tf_op jit(solution)/shard_map/reduce_scatter | solution.py:145
  315.2 1.8 add_convert_fusion
  (67 shorter events, 0.6 us)
Async XLA Ops:
  7.2 14.4 %copy-start = (bf16[256,4096]{1,0:T(8,128)(2,1)S(1)}, bf16[256,4096]{1,0:T(8,128)(2,1)}, u32[]{:S(2)}) copy-start(bf16[256,4096]{1,0:T(8,128)(2,1)} %param.38) | copy-start | bytes 6291460
  7.2 53.6 %all-reduce.4.cloned.1.call-start = ((), (), s32[]{:S(2)}) async-start(), calls=%async_computation.3 | async-start | bytes 1572864 | tf_op jit(solution)/shard_map/psum | solution.py:130
  8.0 3.9 %copy-start.14 = (f32[4096]{0:T(1024)S(1)}, f32[4096]{0:T(1024)}, u32[]{:S(2)}) copy-start(f32[4096]{0:T(1024)} %param.26) | copy-start | bytes 49156
  9.4 5.1 %copy-start.2 = (f32[1,96,1024]{1,2,0:T(8,128)}, f32[1,96,1024]{1,2,0:T(8,128)S(1)}, u32[]{:S(2)}) copy-start(f32[1,96,1024]{1,2,0:T(8,128)S(1)} %copy.42) | copy-start | bytes 1179652
  10.4 4.0 %copy-start.9 = (f32[16,64]{1,0:T(8,128)S(1)}, f32[16,64]{1,0:T(8,128)}, u32[]{:S(2)}) copy-start(f32[16,64]{1,0:T(8,128)} %param.30) | copy-start | bytes 12292
  10.4 4.0 %copy-start.10 = (f32[16,64]{1,0:T(8,128)S(1)}, f32[16,64]{1,0:T(8,128)}, u32[]{:S(2)}) copy-start(f32[16,64]{1,0:T(8,128)} %param.29) | copy-start | bytes 12292
  10.4 4.1 %copy-start.4 = (f32[16,64,16]{1,2,0:T(8,128)S(1)}, f32[16,64,16]{1,2,0:T(8,128)}, u32[]{:S(2)}) copy-start(f32[16,64,16]{1,2,0:T(8,128)} %param.33) | copy-start | bytes 196612
  10.4 4.1 %copy-start.5 = (f32[16,64,16]{1,2,0:T(8,128)S(1)}, f32[16,64,16]{1,2,0:T(8,128)}, u32[]{:S(2)}) copy-start(f32[16,64,16]{1,2,0:T(8,128)} %param.32) | copy-start | bytes 196612
  14.3 4.1 %copy-start.12 = (f32[256]{0:T(256)S(1)}, f32[256]{0:T(256)}, u32[]{:S(2)}) copy-start(f32[256]{0:T(256)} %param.36) | copy-start | bytes 3076
  21.4 1.5 copy-start.13
  22.9 39.7 %copy-start.7 = (f32[4096]{0:T(1024)S(1)}, f32[4096]{0:T(1024)}, u32[]{:S(2)}) copy-start(f32[4096]{0:T(1024)} %param.27) | copy-start | bytes 49156
  22.9 91.1 %all-gather.5.cloned.1.call-start = ((), (), s32[]{:S(2)}) async-start(), calls=%async_computation.6 | async-start | bytes 1769472 | tf_op jit(solution)/shard_map/all_gather | solution.py:137
  62.6 3.4 %copy-start.3 = (bf16[96,4096]{1,0:T(8,128)(2,1)}, bf16[96,4096]{1,0:T(8,128)(2,1)S(1)}, u32[]{:S(2)}) copy-start(bf16[96,4096]{1,0:T(8,128)(2,1)S(1)} %get-tuple-element.4) | copy-start | bytes 2359300
  63.6 78.9 %all-gather.3.cloned.1.call-start = ((), (), s32[]{:S(2)}) async-start(), calls=%async_computation.4 | async-start | bytes 3932160 | tf_op jit(solution)/shard_map/all_gather | solution.py:165
  96.9 103.5 %all-reduce.6.cloned.1.call-start = ((), (), s32[]{:S(2)}) async-start(), calls=%async_computation.7 | async-start | bytes 4718592 | tf_op jit(solution)/shard_map/psum | solution.py:141
  120.4 120.2 %reduce-scatter.3.cloned.1.call-start = ((), (), s32[]{:S(2)}) async-start(), calls=%async_computation.5 | async-start | bytes 3932160 | tf_op jit(solution)/shard_map/reduce_scatter | solution.py:84
  164.2 151.1 %reduce-scatter.5.cloned.1.call-start = ((), (), s32[]{:S(2)}) async-start(), calls=%async_computation.8 | async-start | bytes 1769472 | tf_op jit(solution)/shard_map/reduce_scatter | solution.py:145
  202.7 4.3 %copy-start.8 = (f32[96,2]{0,1:T(2,128)S(1)}, f32[96,2]{0,1:T(2,128)}, u32[]{:S(2)}) copy-start(f32[96,2]{0,1:T(2,128)} %param.40) | copy-start | bytes 2308
  202.7 5.0 %copy-start.11 = (bf16[4096]{0:T(1024)(128)(2,1)S(1)}, bf16[4096]{0:T(1024)(128)(2,1)}, u32[]{:S(2)}) copy-start(bf16[4096]{0:T(1024)(128)(2,1)} %param.47) | copy-start | bytes 24580
  242.1 8.1 %collective-permute-start = (bf16[1,48,1024]{2,1,0:T(8,128)(2,1)S(1)}, bf16[1,48,1024]{2,1,0:T(8,128)(2,1)S(1)}, u32[]{:S(2)}, u32[]{:S(2)}) collective-permute-start(bf16[1,48,1024]{2,1,0:T(8,128)(2,1)S(1)} %get-tuple-element.11), channel_id=1, source_target_pairs={{0,28},{4,0},{8,4},{12,8},{16,12},{20,16},{24,20},{28,24},{1,29},{... | collective-permute-start | bytes 294920 | tf_op jit(solution)/shard_map/ppermute | solution.py:19
  246.7 5.9 %collective-permute-start.1 = (bf16[1,48,1024]{2,1,0:T(8,128)(2,1)S(1)}, bf16[1,48,1024]{2,1,0:T(8,128)(2,1)S(1)}, u32[]{:S(2)}, u32[]{:S(2)}) collective-permute-start(bf16[1,48,1024]{2,1,0:T(8,128)(2,1)S(1)} %get-tuple-element.10), channel_id=1, source_target_pairs={{0,24},{4,28},{8,0},{12,4},{16,8},{20,12},{24,16},{28,20},{1,25},{... | collective-permute-start | bytes 294920 | tf_op jit(solution)/shard_map/ppermute | solution.py:19
  247.2 8.7 %collective-permute-start.2 = (bf16[1,48,1024]{2,1,0:T(8,128)(2,1)S(1)}, bf16[1,48,1024]{2,1,0:T(8,128)(2,1)S(1)}, u32[]{:S(2)}, u32[]{:S(2)}) collective-permute-start(bf16[1,48,1024]{2,1,0:T(8,128)(2,1)S(1)} %get-tuple-element.9), channel_id=1, source_target_pairs={{0,20},{4,24},{8,28},{12,0},{16,4},{20,8},{24,12},{28,16},{1,21},{... | collective-permute-start | bytes 294920 | tf_op jit(solution)/shard_map/ppermute | solution.py:19
  247.2 21.6 %collective-permute-start.3 = (bf16[1,48,1024]{2,1,0:T(8,128)(2,1)S(1)}, bf16[1,48,1024]{2,1,0:T(8,128)(2,1)S(1)}, u32[]{:S(2)}, u32[]{:S(2)}) collective-permute-start(bf16[1,48,1024]{2,1,0:T(8,128)(2,1)S(1)} %get-tuple-element.8), channel_id=1, source_target_pairs={{0,16},{4,20},{8,24},{12,28},{16,0},{20,4},{24,8},{28,12},{1,17},{... | collective-permute-start | bytes 294920 | tf_op jit(solution)/shard_map/ppermute | solution.py:19
  250.2 22.7 %collective-permute-start.4 = (bf16[1,48,1024]{2,1,0:T(8,128)(2,1)S(1)}, bf16[1,48,1024]{2,1,0:T(8,128)(2,1)S(1)}, u32[]{:S(2)}, u32[]{:S(2)}) collective-permute-start(bf16[1,48,1024]{2,1,0:T(8,128)(2,1)S(1)} %get-tuple-element.7), channel_id=1, source_target_pairs={{0,12},{4,16},{8,20},{12,24},{16,28},{20,0},{24,4},{28,8},{1,13},{... | collective-permute-start | bytes 294920 | tf_op jit(solution)/shard_map/ppermute | solution.py:19
  250.2 22.7 %collective-permute-start.5 = (bf16[1,48,1024]{2,1,0:T(8,128)(2,1)S(1)}, bf16[1,48,1024]{2,1,0:T(8,128)(2,1)S(1)}, u32[]{:S(2)}, u32[]{:S(2)}) collective-permute-start(bf16[1,48,1024]{2,1,0:T(8,128)(2,1)S(1)} %get-tuple-element.6), channel_id=1, source_target_pairs={{0,8},{4,12},{8,16},{12,20},{16,24},{20,28},{24,0},{28,4},{1,9},{5... | collective-permute-start | bytes 294920 | tf_op jit(solution)/shard_map/ppermute | solution.py:19
  252.6 20.4 %collective-permute-start.6 = (bf16[1,48,1024]{2,1,0:T(8,128)(2,1)S(1)}, bf16[1,48,1024]{2,1,0:T(8,128)(2,1)S(1)}, u32[]{:S(2)}, u32[]{:S(2)}) collective-permute-start(bf16[1,48,1024]{2,1,0:T(8,128)(2,1)S(1)} %get-tuple-element.5), channel_id=1, source_target_pairs={{0,4},{4,8},{8,12},{12,16},{16,20},{20,24},{24,28},{28,0},{1,5},{5... | collective-permute-start | bytes 294920 | tf_op jit(solution)/shard_map/ppermute | solution.py:19
  273.3 1.5 copy-start.6
  273.3 43.8 %copy-start.1 = (bf16[256,4096]{1,0:T(8,128)(2,1)S(1)}, bf16[256,4096]{1,0:T(8,128)(2,1)}, u32[]{:S(2)}) copy-start(bf16[256,4096]{1,0:T(8,128)(2,1)} %param.38) | copy-start | bytes 6291460
Sparse Core Ops, SparseCore 0:
  23.1 37.7 all-reduce.3
  63.7 50.2 all-gather.4
  115.6 26.8 all-gather.2
  144.7 55.6 all-reduce.5
  202.8 37.7 reduce-scatter.2
  243.9 71.3 reduce-scatter.4
